TPU v7x, 256 devices: a whole 4x4x8 slice. The times are simulated.
256 devices in a mesh: sp: 32 (over z, x), tp: 8 (over y, core).
Axes of the slice: x: 4, y: 4, z: 8, core: 2. Of those that a mesh axis runs over, the one named last changes fastest.
Arguments:
- residual: bfloat16 [10240, 2048], P(('sp', 'tp')), may hold values from -6 to 6
- query_narrow: bfloat16 [10240, 1024], P('sp', 'tp'), may hold values from -48 to 48
- key_narrow: bfloat16 [10240, 1024], P('sp', 'tp'), may hold values from -48 to 48
- value_narrow: bfloat16 [10240, 1024], P('sp', 'tp'), may hold values from -6 to 6
- query_wide: bfloat16 [10240, 2048], P('sp', 'tp'), may hold values from -48 to 48
- key_wide: bfloat16 [10240, 2048], P('sp', 'tp'), may hold values from -48 to 48
- value_wide: bfloat16 [10240, 1024], P('sp', 'tp'), may hold values from -6 to 6
- subtract_narrow: float32 [8], P('tp'), may hold values from 0.3 to 0.8
- subtract_wide: float32 [8], P('tp'), may hold values from 0.3 to 0.8
- head_gain: float32 [128], replicated, may hold values from 0.1 to 1.9
- out_narrow: bfloat16 [1024, 2048], replicated, may hold values from -0.125 to 0.125
- out_wide: bfloat16 [1024, 2048], replicated, may hold values from -0.125 to 0.125
- norm1_gain: float32 [2048], replicated, may hold values from 0.1 to 1.9
- norm2_gain: float32 [2048], replicated, may hold values from 0.1 to 1.9
- expert_ids: int32 [10240, 2], P(('sp', 'tp')), may hold values from 0 to 31, all different within a row; in each aligned block of 40 rows (0 to 39, 40 to 79, ...) at most 3 rows name the same one
- expert_weight: float32 [10240, 2], P(('sp', 'tp')), may hold values from 0.1 to 1
- gate_proj: bfloat16 [32, 2048, 2048], P('sp', None, 'tp'), may hold values from -0.125 to 0.125
- up_proj: bfloat16 [32, 2048, 2048], P('sp', None, 'tp'), may hold values from -0.125 to 0.125
- down_proj: bfloat16 [32, 2048, 2048], P('sp', 'tp'), may hold values from -0.125 to 0.125
Outputs:
- layer_out: bfloat16 [10240, 2048], P(('sp', 'tp'))
Inputs may be any that keep to these rules, and one draw needn't show every extreme that they name: `expert_ids`: each row names 2 different experts. Among the 40 rows of one device no expert is named more than 3 times, and in some device's rows some expert is named exactly 3 times.
All inputs are finite; a program needn't handle non-finite values.
Results may differ from a plain program's by a relative error of at most 0.014.
Values may be sent and summed in bfloat16 or wider, within the bound.
A program may use at most 128 MiB of HBM per device.

v0:
```python
import jax
import jax.numpy as jnp
from jax import lax
from jax.sharding import PartitionSpec as P

residual_scale = 2.0**0.5


def in_one_piece(arrays, axis, dim, along):
    ends, at = ([], 0)
    for a in arrays[:-1]:
        at += a.shape[along]
        ends.append(at)
    both = jnp.concatenate(arrays, axis=along)
    return tuple(jnp.split(lax.all_gather(both, axis, axis=dim, tiled=True), ends, axis=along))


def in_blocks(value, dim, devices):
    before, after = (value.shape[:dim], value.shape[dim + 1 :])
    return jnp.moveaxis(value.reshape(*before, devices, -1, *after), dim, 0)


def sent_and_summed(value, axis, dim):
    devices = lax.axis_size(axis)
    pieces = lax.all_to_all(in_blocks(value, dim, devices), axis, 0, 0, tiled=True)
    return jnp.sum(pieces.astype(jnp.float32), axis=0)


def items_in_groups(value, axis, split_dim, concat_dim, work, item_dim, out_dim):
    items = jax.tree.leaves(value)[0].shape[item_dim]
    count = 2 if items % 2 == 0 else 1
    outs = []
    for k in range(count):
        group = jax.tree.map(
            lambda a: lax.slice_in_dim(
                a, k * (items // count), (k + 1) * (items // count), axis=item_dim
            ),
            value,
        )
        outs.append(
            work(
                lax.all_to_all(
                    group, axis, split_axis=split_dim, concat_axis=concat_dim, tiled=True
                )
            )
        )
    return jax.tree.map(lambda *parts: jnp.concatenate(parts, axis=out_dim), *outs)


def layer_norm(values, gain):
    center = jnp.mean(values, -1, keepdims=True)
    spread = jnp.mean(jnp.square(values - center), -1, keepdims=True)
    return (values - center) * lax.rsqrt(spread + 1e-05) * gain


def block_take(shards, shard_rows):
    take = shards
    for count in range(shards, 0, -1):
        if shards % count == 0 and count * shard_rows >= 512:
            take = count
    return take


def start_carry(head_count, tok_rows, value_size):
    return (
        jnp.full((head_count, 2, tok_rows), -1e30, jnp.float32),
        jnp.zeros((head_count, 2, tok_rows), jnp.float32),
        jnp.zeros((head_count, 2, tok_rows, value_size), jnp.float32),
    )


def absorb_keys(carry, queries, key_piece, value_piece, shard_rows):
    head_count = queries.shape[1]
    key_size = queries.shape[3]
    shards = key_piece.shape[0] // shard_rows
    take = block_take(shards, shard_rows)
    span = take * shard_rows

    def one_block(step_index, state):
        rowtop, total, summed = state
        key_block = lax.dynamic_slice_in_dim(key_piece, step_index * span, span, 0).reshape(
            span, head_count, 2, key_size
        )
        value_block = lax.dynamic_slice_in_dim(value_piece, step_index * span, span, 0).reshape(
            span, head_count, -1
        )
        scores = jnp.einsum(
            "qhmd,khmd->hmqk", queries, key_block, preferred_element_type=jnp.float32
        ) * key_size ** (-0.5)
        newtop = jnp.maximum(rowtop, jnp.max(scores, -1))
        shrink = jnp.exp(rowtop - newtop)
        expo = jnp.exp(scores - newtop[..., None])
        total = total * shrink + jnp.sum(expo, -1)
        summed = summed * shrink[..., None] + jnp.einsum(
            "hmqk,khe->hmqe",
            expo.astype(jnp.bfloat16),
            value_block,
            preferred_element_type=jnp.float32,
        )
        return (newtop, total, summed)

    return lax.fori_loop(0, shards // take, one_block, carry)


def finish_heads(carry, subtract, head_gain):
    rowtop, total, summed = carry
    mapped = summed / total[..., None]
    diff = mapped[:, 0] - subtract[:, None, None] * mapped[:, 1]
    normed = diff * lax.rsqrt(jnp.mean(diff * diff, -1, keepdims=True) + 1e-06) * head_gain
    return jnp.transpose(normed, (1, 0, 2)).reshape(diff.shape[1], -1).astype(jnp.bfloat16)


def on_device(
    residual,
    query_narrow,
    key_narrow,
    value_narrow,
    query_wide,
    key_wide,
    value_wide,
    subtract_narrow,
    subtract_wide,
    head_gain,
    out_narrow,
    out_wide,
    norm1_gain,
    norm2_gain,
    expert_ids,
    expert_weight,
    gate_proj,
    up_proj,
    down_proj,
):
    tok_rows = query_narrow.shape[0]
    head_count = subtract_narrow.shape[0]
    value_size = head_gain.shape[0]
    narrow_queries = query_narrow.reshape(tok_rows, head_count, 2, -1)
    wide_queries = query_wide.reshape(tok_rows, head_count, 2, -1)
    narrow_start = start_carry(head_count, tok_rows, value_size)
    wide_start = start_carry(head_count, tok_rows, value_size)
    pieces = in_one_piece((key_narrow, value_narrow), "sp", 0, 1)
    narrow_state = absorb_keys(narrow_start, narrow_queries, pieces[0], pieces[1], tok_rows)
    pieces = in_one_piece((key_wide, value_wide), "sp", 0, 1)
    wide_state = absorb_keys(wide_start, wide_queries, pieces[0], pieces[1], tok_rows)
    attended_narrow = finish_heads(narrow_state, subtract_narrow, head_gain)
    attended_wide = finish_heads(wide_state, subtract_wide, head_gain)
    offset = lax.axis_index("tp") * head_count * value_size
    local_narrow = lax.dynamic_slice_in_dim(out_narrow, offset, head_count * value_size, 0)
    local_wide = lax.dynamic_slice_in_dim(out_wide, offset, head_count * value_size, 0)
    mix = sent_and_summed(
        (
            jnp.dot(attended_narrow, local_narrow, preferred_element_type=jnp.float32)
            + jnp.dot(attended_wide, local_wide, preferred_element_type=jnp.float32)
        ).astype(jnp.bfloat16),
        "tp",
        0,
    )
    hidden = layer_norm(residual_scale * residual.astype(jnp.float32) + mix, norm1_gain).astype(
        jnp.bfloat16
    )
    local_rows, top_count = expert_ids.shape
    experts = lax.axis_size("sp")
    capacity = max(2, 3 * local_rows * top_count // (2 * experts))
    flat_ids = expert_ids.reshape(-1)
    onehot = (flat_ids[:, None] == jnp.arange(experts, dtype=jnp.int32)[None, :]).astype(jnp.int32)
    before = jnp.cumsum(onehot, 0) - onehot
    position = jnp.sum(before * onehot, 1)
    slots = (flat_ids * capacity + position).reshape(local_rows, top_count)
    dispatch_table = jnp.any(
        jnp.arange(experts * capacity, dtype=jnp.int32)[:, None, None] == slots[None], -1
    ).astype(jnp.bfloat16)
    outgoing = jnp.dot(dispatch_table, hidden, preferred_element_type=jnp.float32).astype(
        jnp.bfloat16
    )
    outgoing = outgoing.reshape(experts, capacity, -1)

    def run_expert(received):
        gathered = lax.all_gather(received, "tp", axis=1, tiled=True)
        flat_rows = gathered.reshape(-1, gathered.shape[2])
        gate_part = jnp.dot(flat_rows, gate_proj[0], preferred_element_type=jnp.float32)
        up_part = jnp.dot(flat_rows, up_proj[0], preferred_element_type=jnp.float32)
        inner = (jax.nn.silu(gate_part) * up_part).astype(jnp.bfloat16)
        partial_out = jnp.dot(inner, down_proj[0], preferred_element_type=jnp.float32).reshape(
            gathered.shape
        )
        summed = lax.psum_scatter(
            partial_out.astype(jnp.bfloat16), "tp", scatter_dimension=1, tiled=True
        )
        return lax.all_to_all(summed, "sp", split_axis=0, concat_axis=0, tiled=True)

    returned = items_in_groups(outgoing, "sp", 0, 0, run_expert, 1, 1)
    returned_flat = returned.reshape(experts * capacity, -1)
    picked = returned_flat[slots].astype(jnp.float32)
    routed = jnp.sum(expert_weight[..., None] * picked, 1)
    return layer_norm(residual_scale * hidden.astype(jnp.float32) + routed, norm2_gain).astype(
        jnp.bfloat16
    )


def solution(mesh):
    placed = (
        P(("sp", "tp"), None),
        P("sp", "tp"),
        P("sp", "tp"),
        P("sp", "tp"),
        P("sp", "tp"),
        P("sp", "tp"),
        P("sp", "tp"),
        P("tp"),
        P("tp"),
        P(),
        P(),
        P(),
        P(),
        P(),
        P(("sp", "tp"), None),
        P(("sp", "tp"), None),
        P("sp", None, "tp"),
        P("sp", None, "tp"),
        P("sp", "tp", None),
    )
    return jax.shard_map(
        on_device, mesh=mesh, in_specs=placed, out_specs=P(("sp", "tp"), None), check_vma=False
    )
```

profile of v0, /device:TPU:25, one launch (start us, length us, event | category | flops | bytes accessed | tf_op | source)
XLA Modules:
  0.0 422.1 jit_solution(8756736317949425885)
XLA Ops:
  6.5 1.7 pad_maximum_fusion.1
  8.3 1.7 pad_maximum_fusion
  10.1 1.6 copy.88
  14.7 79.7 %all-gather.4.cloned.1.call-done = bf16[10240,256]{1,0:T(8,128)(2,1)} async-done(((bf16[320,256]{1,0:T(8,128)(2,1)}), bf16[10240,256]{1,0:T(8,128)(2,1)}) %all-gather.4.cloned.1.call-update) | async-done | bytes 5242896 | tf_op jit(solution)/shard_map/all_gather | solution.py:15
  94.4 4.1 fusion.57
  98.5 72.0 %while.36 = (s32[]{:T(128)}, f32[1,2,320]{2,1,0:T(2,128)S(1)}, f32[1,2,320]{2,1,0:T(2,128)S(1)}, f32[1,2,320,128]{3,2,1,0:T(8,128)S(1)}, bf16[10240,128]{1,0:T(8...) while((s32[]{:T(128)}, f32[1,2,320]{2,1,0:T(2,128)S(1)}, ...), condition=%wide.region_3.0_spmd.clone, body=%wide.region_0.0_spmd.clone.sunk | while | flops 160812800 | bytes 6676655 | solution.py:102
  159.5 1.5 fusion.82
  170.8 3.1 fusion.35
  173.9 17.8 %all-gather.6.cloned.1.call-done = bf16[10240,384]{1,0:T(8,128)(2,1)} async-done(((bf16[320,384]{1,0:T(8,128)(2,1)}), bf16[10240,384]{1,0:T(8,128)(2,1)}) %all-gather.6.cloned.1.call-update) | async-done | bytes 7864336 | tf_op jit(solution)/shard_map/all_gather | solution.py:15
  191.6 4.2 split.18
  195.8 2.9 split.19
  198.8 58.4 %while.37 = (s32[]{:T(128)}, f32[1,2,320]{2,1,0:T(2,128)S(1)}, f32[1,2,320]{2,1,0:T(2,128)S(1)}, f32[1,2,320,128]{3,2,1,0:T(8,128)S(1)}, bf16[10240,256]{1,0:T(8...) while((s32[]{:T(128)}, f32[1,2,320]{2,1,0:T(2,128)S(1)}, ...), condition=%wide.region_8.0_spmd.clone, body=%wide.region_5.8_spmd.clone.sunk | while | flops 213241600 | bytes 7577775 | solution.py:102
  257.5 3.5 fusion.28
  261.0 6.1 %all-to-all-start = ((bf16[8,40,2048]{2,1,0:T(8,128)(2,1)}), bf16[8,40,2048]{2,1,0:T(8,128)(2,1)S(1)}, u32[]{:S(2)}, u32[]{:S(2)}) async-start(bf16[8,40,2048]{2,1,0:T(8,128)(2,1)} %bitcast.7), calls=%async_computation | async-start | bytes 2621440 | tf_op jit(solution)/shard_map/all_to_all | solution.py:25
  268.0 15.2 %all-to-all-done = bf16[8,40,2048]{2,1,0:T(8,128)(2,1)S(1)} async-done(((bf16[8,40,2048]{2,1,0:T(8,128)(2,1)}), bf16[8,40,2048]{2,1,0:T(8,128)(2,1)S(1)}, u32[]{:S(2)}, u32[]{:S(2)}) %all-to-all-start) | async-done | bytes 1310752 | tf_op jit(solution)/shard_map/all_to_all | solution.py:25
  284.4 20.4 %all_to_all.15 = bf16[32,3,2048]{2,1,0:T(4,128)(2,1)S(1)} all-to-all(bf16[32,3,2048]{2,1,0:T(4,128)(2,1)S(1)} %reshape.302), channel_id=1, replica_groups=mesh['sp'=32,'tp'=8] {'sp'}, dimensions={0} | all-to-all | bytes 786432 | tf_op jit(solution)/shard_map/all_to_all | solution.py:42
  306.1 28.0 %all-gather.8.cloned.1.call-done = bf16[32,24,2048]{2,0,1:T(8,128)(2,1)} async-done(((bf16[32,3,2048]{2,0,1:T(8,128)(2,1)}), bf16[32,24,2048]{2,0,1:T(8,128)(2,1)}) %all-gather.8.cloned.1.call-update) | async-done | bytes 3145744 | tf_op jit(solution)/shard_map/all_gather | solution.py:178
  334.1 3.6 copy.96
  337.8 2.3 fusion.32
  342.1 3.4 copy.97
  345.5 37.9 %reduce-scatter.2.cloned.1.call-done = bf16[32,3,2048]{2,0,1:T(8,128)(2,1)} async-done(((bf16[32,24,2048]{2,0,1:T(8,128)(2,1)}), bf16[32,3,2048]{2,0,1:T(8,128)(2,1)}) %reduce-scatter.2.cloned.1.call-update) | async-done | bytes 393232 | tf_op jit(solution)/shard_map/reduce_scatter | solution.py:186
  383.4 2.1 copy.98
  385.5 9.2 %all-to-all-start.2 = ((bf16[32,3,2048]{2,1,0:T(4,128)(2,1)}), bf16[32,3,2048]{2,1,0:T(4,128)(2,1)S(1)}, u32[]{:S(2)}, u32[]{:S(2)}) async-start(bf16[32,3,2048]{2,1,0:T(4,128)(2,1)} %copy.98), calls=%async_computation.3 | async-start | bytes 1048576 | tf_op jit(solution)/shard_map/all_to_all | solution.py:189
  395.0 16.9 %all-to-all-done.2 = bf16[32,3,2048]{2,1,0:T(4,128)(2,1)S(1)} async-done(((bf16[32,3,2048]{2,1,0:T(4,128)(2,1)}), bf16[32,3,2048]{2,1,0:T(4,128)(2,1)S(1)}, u32[]{:S(2)}, u32[]{:S(2)}) %all-to-all-start.2) | async-done | bytes 393248 | tf_op jit(solution)/shard_map/all_to_all | solution.py:189
  (328 shorter events, 138.9 us)
Async XLA Ops:
  6.5 334.5 %copy-start = (bf16[1,256,2048]{2,1,0:T(8,128)(2,1)S(1)}, bf16[1,256,2048]{2,1,0:T(8,128)(2,1)}, u32[]{:S(2)}) copy-start(bf16[1,256,2048]{2,1,0:T(8,128)(2,1)} %param.41) | copy-start | bytes 3145732
  6.5 87.8 %all-gather.4.cloned.1.call-start = ((), (), s32[]{:S(2)}) async-start(), calls=%async_computation.4 | async-start | bytes 5406720 | tf_op jit(solution)/shard_map/all_gather | solution.py:15
  8.3 183.4 %all-gather.6.cloned.1.call-start = ((), (), s32[]{:S(2)}) async-start(), calls=%async_computation.5 | async-start | bytes 8110080 | tf_op jit(solution)/shard_map/all_gather | solution.py:15
  98.5 72.3 %copy-start.6 = (f32[128]{0:T(128)S(1)}, f32[128]{0:T(128)}, u32[]{:S(2)}) copy-start(f32[128]{0:T(128)} %param.32) | copy-start | bytes 1540
  195.8 2.9 copy-start.1
  257.5 9.6 %copy-start.5 = (s32[40,2]{0,1:T(2,128)S(1)}, s32[40,2]{0,1:T(2,128)}, u32[]{:S(2)}) copy-start(s32[40,2]{0,1:T(2,128)} %param.37) | copy-start | bytes 964
  261.0 22.4 %copy-start.2 = (bf16[40,2048]{1,0:T(8,128)(2,1)S(1)}, bf16[40,2048]{1,0:T(8,128)(2,1)}, u32[]{:S(2)}) copy-start(bf16[40,2048]{1,0:T(8,128)(2,1)} %param.23) | copy-start | bytes 491524
  261.0 22.7 %copy-start.3 = (f32[2048]{0:T(1024)S(1)}, f32[2048]{0:T(1024)}, u32[]{:S(2)}) copy-start(f32[2048]{0:T(1024)} %param.35) | copy-start | bytes 24580
  261.0 22.2 %all-to-all-start = ((bf16[8,40,2048]{2,1,0:T(8,128)(2,1)}), bf16[8,40,2048]{2,1,0:T(8,128)(2,1)S(1)}, u32[]{:S(2)}, u32[]{:S(2)}) async-start(bf16[8,40,2048]{2,1,0:T(8,128)(2,1)} %bitcast.7), calls=%async_computation | async-start | bytes 2621440 | tf_op jit(solution)/shard_map/all_to_all | solution.py:25
  267.1 67.1 %all-gather.8.cloned.1.call-start = ((), (), s32[]{:S(2)}) async-start(), calls=%async_computation.6 | async-start | bytes 3538944 | tf_op jit(solution)/shard_map/all_gather | solution.py:178
  305.9 77.5 %reduce-scatter.2.cloned.1.call-start = ((), (), s32[]{:S(2)}) async-start(), calls=%async_computation.7 | async-start | bytes 3538944 | tf_op jit(solution)/shard_map/reduce_scatter | solution.py:186
  337.7 2.3 copy-start.8
  345.5 49.5 %copy-start.7 = (f32[40,2]{0,1:T(2,128)S(1)}, f32[40,2]{0,1:T(2,128)}, u32[]{:S(2)}) copy-start(f32[40,2]{0,1:T(2,128)} %param.38) | copy-start | bytes 964
  385.5 26.4 %all-to-all-start.2 = ((bf16[32,3,2048]{2,1,0:T(4,128)(2,1)}), bf16[32,3,2048]{2,1,0:T(4,128)(2,1)S(1)}, u32[]{:S(2)}, u32[]{:S(2)}) async-start(bf16[32,3,2048]{2,1,0:T(4,128)(2,1)} %copy.98), calls=%async_computation.3 | async-start | bytes 1048576 | tf_op jit(solution)/shard_map/all_to_all | solution.py:189
  412.2 2.6 copy-start.4
Sparse Core Ops, SparseCore 0:
  9.9 84.4 all-gather.3
  97.0 94.6 all-gather.5
  306.0 28.0 all-gather.7
  345.6 37.7 reduce-scatter.1
where the time goes:
time: 425 us; the launch traced here: 422 us
  waiting for transfers between devices  195 us (46%)
  matrix products  87.6 us (21%)
  local copies, waits for them, and re-layouts  64.1 us (15%)
  other arithmetic  22.6 us (5%)
  blocking collectives  20.4 us (5%)
  starting transfers between devices  15.5 us (4%)
  between operations  14.7 us (3%)
    all_gather x2, waiting for transfers between devices, in_one_piece(): lax.all_gather(both, axis, axis=dim, tiled=True)  97.4 us
    dot_general x32, matrix products, one_block(): jnp.einsum('hmqk,khe->hmqe', expo.astype(jnp.bfloat16), value_block, pref...  46.3 us
    reduce_scatter x1, waiting for transfers between devices, run_expert(): lax.psum_scatter(partial_out.astype(jnp.bfloat16), 'tp', scatter_dimensio...  37.9 us
    dynamic_slice x64, local copies, waits for them, and re-layouts, one_block(): lax.dynamic_slice_in_dim(key_piece, step_index * span, span, 0)  36.8 us
    dot_general x32, matrix products, one_block(): jnp.einsum('qhmd,khmd->hmqk', queries, key_block, preferred_element_type=...  30.2 us
    all_gather x1, waiting for transfers between devices, run_expert(): gathered = lax.all_gather(received, 'tp', axis=1, tiled=True)  28 us
    all_to_all x1, blocking collectives, items_in_groups(): lax.all_to_all(group, axis, split_axis=split_dim, concat_axis=concat_dim,...  20.4 us
    all_to_all x1, waiting for transfers between devices, run_expert(): return lax.all_to_all(summed, 'sp', split_axis=0, concat_axis=0, tiled=True)  16.9 us
  transfers between devices with their start and end apart: 6, of which 6 were waited for; matrix products, arithmetic and copies ran while one was open for 20% of the time, Pallas kernels for 0%

commit v1 on v0

--- a/solution.py
+++ b/solution.py
@@ -175,7 +175,9 @@
     outgoing = outgoing.reshape(experts, capacity, -1)
 
     def run_expert(received):
-        gathered = lax.all_gather(received, "tp", axis=1, tiled=True)
+        gathered = jnp.concatenate(
+            lax.all_to_all(jnp.stack([received] * lax.axis_size("tp")), "tp", 0, 0), axis=1
+        )
         flat_rows = gathered.reshape(-1, gathered.shape[2])
         gate_part = jnp.dot(flat_rows, gate_proj[0], preferred_element_type=jnp.float32)
         up_part = jnp.dot(flat_rows, up_proj[0], preferred_element_type=jnp.float32)

time: 425 us -> 446 us (1.049)
  blocking collectives: 20.4 us -> 63.6 us
  waiting for transfers between devices: 195 us -> 163 us
  local copies, waits for them, and re-layouts: 64.1 us -> 73.7 us
    all_to_all x0 -> x1, blocking collectives: none -> 43.2 us  [run_expert(): lax.all_to_all(jnp.stack([received] * lax.axis_size('tp')), 'tp', 0, 0)]
    all_gather x1 -> x0, waiting for transfers between devices: 28 us -> none  [run_expert(): gathered = lax.all_gather(received, 'tp', axis=1, tiled=True)]
    another operation x0 -> x2, local copies, waits for them, and re-layouts: none -> 9.19 us  [the longest x1 8.81 us: run_expert(): flat_rows = gathered.reshape(-1, gathered.shape[2])]
    reshape x0 -> x1, local copies, waits for them, and re-layouts: none -> 4.63 us  [run_expert(): jnp.concatenate(lax.all_to_all(jnp.stack([received] * lax.axis_size('tp')...]
  transfers between devices with their start and end apart: 6 -> 5, of which waited for: 6 -> 5; matrix products, arithmetic and copies ran while one was open for 20% -> 19% of each run, Pallas kernels for 0% -> 0%
where the time goes in v1:
time: 446 us; the launch traced here: 443 us
  waiting for transfers between devices  163 us (37%)
  matrix products  88.7 us (20%)
  local copies, waits for them, and re-layouts  73.7 us (17%)
  blocking collectives  63.6 us (14%)
  other arithmetic  22.6 us (5%)
  starting transfers between devices  15.3 us (3%)
  between operations  14.7 us (3%)
    all_gather x2, waiting for transfers between devices, in_one_piece(): lax.all_gather(both, axis, axis=dim, tiled=True)  97.4 us
    dot_general x32, matrix products, one_block(): jnp.einsum('hmqk,khe->hmqe', expo.astype(jnp.bfloat16), value_block, pref...  46.3 us
    all_to_all x1, blocking collectives, run_expert(): lax.all_to_all(jnp.stack([received] * lax.axis_size('tp')), 'tp', 0, 0)  43.2 us
    dynamic_slice x64, local copies, waits for them, and re-layouts, one_block(): lax.dynamic_slice_in_dim(key_piece, step_index * span, span, 0)  36.8 us
    reduce_scatter x1, waiting for transfers between devices, run_expert(): lax.psum_scatter(partial_out.astype(jnp.bfloat16), 'tp', scatter_dimensio...  33.5 us
    dot_general x32, matrix products, one_block(): jnp.einsum('qhmd,khmd->hmqk', queries, key_block, preferred_element_type=...  30.2 us
    all_to_all x1, blocking collectives, items_in_groups(): lax.all_to_all(group, axis, split_axis=split_dim, concat_axis=concat_dim,...  20.4 us
    all_to_all x1, waiting for transfers between devices, run_expert(): return lax.all_to_all(summed, 'sp', split_axis=0, concat_axis=0, tiled=True)  16.9 us
  transfers between devices with their start and end apart: 5, of which 5 were waited for; matrix products, arithmetic and copies ran while one was open for 19% of the time, Pallas kernels for 0%

profile of v1, /device:TPU:25, one launch (start us, length us, event | category | flops | bytes accessed | tf_op | source)
XLA Modules:
  0.0 443.2 jit_solution(13553304272063400973)
XLA Ops:
  6.5 1.7 pad_maximum_fusion.1
  8.3 1.7 pad_maximum_fusion
  10.1 1.6 copy.76
  14.7 79.7 %all-gather.3.cloned.1.call-done = bf16[10240,256]{1,0:T(8,128)(2,1)} async-done(((bf16[320,256]{1,0:T(8,128)(2,1)}), bf16[10240,256]{1,0:T(8,128)(2,1)}) %all-gather.3.cloned.1.call-update) | async-done | bytes 5242896 | tf_op jit(solution)/shard_map/all_gather | solution.py:15
  94.4 4.1 fusion.57
  98.5 72.0 %while.36 = (s32[]{:T(128)}, f32[1,2,320]{2,1,0:T(2,128)S(1)}, f32[1,2,320]{2,1,0:T(2,128)S(1)}, f32[1,2,320,128]{3,2,1,0:T(8,128)S(1)}, bf16[10240,128]{1,0:T(8...) while((s32[]{:T(128)}, f32[1,2,320]{2,1,0:T(2,128)S(1)}, ...), condition=%wide.region_3.0_spmd.clone, body=%wide.region_0.0_spmd.clone.sunk | while | flops 160812800 | bytes 6676655 | solution.py:102
  170.8 3.1 fusion.35
  173.9 17.8 %all-gather.5.cloned.1.call-done = bf16[10240,384]{1,0:T(8,128)(2,1)} async-done(((bf16[320,384]{1,0:T(8,128)(2,1)}), bf16[10240,384]{1,0:T(8,128)(2,1)}) %all-gather.5.cloned.1.call-update) | async-done | bytes 7864336 | tf_op jit(solution)/shard_map/all_gather | solution.py:15
  191.6 4.2 split.18
  195.8 2.9 split.19
  198.8 58.4 %while.37 = (s32[]{:T(128)}, f32[1,2,320]{2,1,0:T(2,128)S(1)}, f32[1,2,320]{2,1,0:T(2,128)S(1)}, f32[1,2,320,128]{3,2,1,0:T(8,128)S(1)}, bf16[10240,256]{1,0:T(8...) while((s32[]{:T(128)}, f32[1,2,320]{2,1,0:T(2,128)S(1)}, ...), condition=%wide.region_8.0_spmd.clone, body=%wide.region_5.8_spmd.clone.sunk | while | flops 213241600 | bytes 7577775 | solution.py:102
  257.5 3.5 fusion.28
  261.0 6.1 %all-to-all-start = ((bf16[8,40,2048]{2,1,0:T(8,128)(2,1)}), bf16[8,40,2048]{2,1,0:T(8,128)(2,1)S(1)}, u32[]{:S(2)}, u32[]{:S(2)}) async-start(bf16[8,40,2048]{2,1,0:T(8,128)(2,1)} %bitcast.7), calls=%async_computation | async-start | bytes 2621440 | tf_op jit(solution)/shard_map/all_to_all | solution.py:25
  268.0 15.2 %all-to-all-done = bf16[8,40,2048]{2,1,0:T(8,128)(2,1)S(1)} async-done(((bf16[8,40,2048]{2,1,0:T(8,128)(2,1)}), bf16[8,40,2048]{2,1,0:T(8,128)(2,1)S(1)}, u32[]{:S(2)}, u32[]{:S(2)}) %all-to-all-start) | async-done | bytes 1310752 | tf_op jit(solution)/shard_map/all_to_all | solution.py:25
  284.4 20.4 %all_to_all.20 = bf16[32,3,2048]{2,1,0:T(4,128)(2,1)S(1)} all-to-all(bf16[32,3,2048]{2,1,0:T(4,128)(2,1)S(1)} %reshape.304), channel_id=1, replica_groups=mesh['sp'=32,'tp'=8] {'sp'}, dimensions={0} | all-to-all | bytes 786432 | tf_op jit(solution)/shard_map/all_to_all | solution.py:42
  305.5 43.2 %all_to_all.21 = bf16[8,32,3,2048]{3,1,2,0:T(8,128)(2,1)S(1)} all-to-all(bf16[8,32,3,2048]{3,1,2,0:T(8,128)(2,1)S(1)} %stack.2), channel_id=1, replica_groups=mesh['sp'=32,'tp'=8] {'tp'}, dimensions={0} | all-to-all | bytes 6291456 | tf_op jit(solution)/shard_map/all_to_all | solution.py:179
  348.7 4.6 %copy.84 = bf16[32,8,3,2048]{3,2,1,0:T(4,128)(2,1)} copy(bf16[32,8,3,2048]{3,0,2,1:T(8,128)(2,1)S(1)} %bitcast.151) | data formatting | bytes 6291456 | tf_op jit(solution)/shard_map/reshape | solution.py:178
  353.3 8.8 %reshape_reshape.3 = bf16[768,2048]{1,0:T(8,128)(2,1)} reshape(bf16[32,8,3,2048]{3,2,1,0:T(4,128)(2,1)} %copy.84) | data formatting | bytes 6291456 | tf_op jit(solution)/shard_map/reshape;reshape | solution.py:181
  362.1 3.3 fusion.32
  367.6 3.4 copy.85
  371.0 33.5 %reduce-scatter.2.cloned.1.call-done = bf16[32,3,2048]{2,0,1:T(8,128)(2,1)} async-done(((bf16[32,24,2048]{2,0,1:T(8,128)(2,1)}), bf16[32,3,2048]{2,0,1:T(8,128)(2,1)}) %reduce-scatter.2.cloned.1.call-update) | async-done | bytes 393232 | tf_op jit(solution)/shard_map/reduce_scatter | solution.py:188
  404.5 2.1 copy.86
  406.6 9.2 %all-to-all-start.3 = ((bf16[32,3,2048]{2,1,0:T(4,128)(2,1)}), bf16[32,3,2048]{2,1,0:T(4,128)(2,1)S(1)}, u32[]{:S(2)}, u32[]{:S(2)}) async-start(bf16[32,3,2048]{2,1,0:T(4,128)(2,1)} %copy.86), calls=%async_computation.4 | async-start | bytes 1048576 | tf_op jit(solution)/shard_map/all_to_all | solution.py:191
  416.1 16.9 %all-to-all-done.3 = bf16[32,3,2048]{2,1,0:T(4,128)(2,1)S(1)} async-done(((bf16[32,3,2048]{2,1,0:T(4,128)(2,1)}), bf16[32,3,2048]{2,1,0:T(4,128)(2,1)S(1)}, u32[]{:S(2)}, u32[]{:S(2)}) %all-to-all-start.3) | async-done | bytes 393248 | tf_op jit(solution)/shard_map/all_to_all | solution.py:191
  (330 shorter events, 139.8 us)
Async XLA Ops:
  6.5 360.0 %copy-start = (bf16[1,256,2048]{2,1,0:T(8,128)(2,1)S(1)}, bf16[1,256,2048]{2,1,0:T(8,128)(2,1)}, u32[]{:S(2)}) copy-start(bf16[1,256,2048]{2,1,0:T(8,128)(2,1)} %param.41) | copy-start | bytes 3145732
  6.5 87.8 %all-gather.3.cloned.1.call-start = ((), (), s32[]{:S(2)}) async-start(), calls=%async_computation.5 | async-start | bytes 5406720 | tf_op jit(solution)/shard_map/all_gather | solution.py:15
  8.3 183.4 %all-gather.5.cloned.1.call-start = ((), (), s32[]{:S(2)}) async-start(), calls=%async_computation.6 | async-start | bytes 8110080 | tf_op jit(solution)/shard_map/all_gather | solution.py:15
  98.5 72.3 %copy-start.7 = (f32[128]{0:T(128)S(1)}, f32[128]{0:T(128)}, u32[]{:S(2)}) copy-start(f32[128]{0:T(128)} %param.32) | copy-start | bytes 1540
  195.8 2.9 copy-start.1
  257.5 9.6 %copy-start.6 = (s32[40,2]{0,1:T(2,128)S(1)}, s32[40,2]{0,1:T(2,128)}, u32[]{:S(2)}) copy-start(s32[40,2]{0,1:T(2,128)} %param.37) | copy-start | bytes 964
  261.0 22.4 %copy-start.3 = (bf16[40,2048]{1,0:T(8,128)(2,1)S(1)}, bf16[40,2048]{1,0:T(8,128)(2,1)}, u32[]{:S(2)}) copy-start(bf16[40,2048]{1,0:T(8,128)(2,1)} %param.23) | copy-start | bytes 491524
  261.0 22.7 %copy-start.4 = (f32[2048]{0:T(1024)S(1)}, f32[2048]{0:T(1024)}, u32[]{:S(2)}) copy-start(f32[2048]{0:T(1024)} %param.35) | copy-start | bytes 24580
  261.0 22.2 %all-to-all-start = ((bf16[8,40,2048]{2,1,0:T(8,128)(2,1)}), bf16[8,40,2048]{2,1,0:T(8,128)(2,1)S(1)}, u32[]{:S(2)}, u32[]{:S(2)}) async-start(bf16[8,40,2048]{2,1,0:T(8,128)(2,1)} %bitcast.7), calls=%async_computation | async-start | bytes 2621440 | tf_op jit(solution)/shard_map/all_to_all | solution.py:25
  267.1 137.4 %reduce-scatter.2.cloned.1.call-start = ((), (), s32[]{:S(2)}) async-start(), calls=%async_computation.7 | async-start | bytes 3538944 | tf_op jit(solution)/shard_map/reduce_scatter | solution.py:188
  362.1 3.3 copy-start.2
  362.1 3.4 copy-start.9
  371.0 45.0 %copy-start.8 = (f32[40,2]{0,1:T(2,128)S(1)}, f32[40,2]{0,1:T(2,128)}, u32[]{:S(2)}) copy-start(f32[40,2]{0,1:T(2,128)} %param.38) | copy-start | bytes 964
  406.6 26.4 %all-to-all-start.3 = ((bf16[32,3,2048]{2,1,0:T(4,128)(2,1)}), bf16[32,3,2048]{2,1,0:T(4,128)(2,1)S(1)}, u32[]{:S(2)}, u32[]{:S(2)}) async-start(bf16[32,3,2048]{2,1,0:T(4,128)(2,1)} %copy.86), calls=%async_computation.4 | async-start | bytes 1048576 | tf_op jit(solution)/shard_map/all_to_all | solution.py:191
  433.3 2.6 copy-start.5
Sparse Core Ops, SparseCore 0:
  9.9 84.4 all-gather.2
  97.0 94.6 all-gather.4
  371.1 33.3 reduce-scatter.1
